TPU v7x, 512 devices: a whole 4x8x8 slice. The times are simulated.
512 devices in a mesh: sp: 64 (over z, y), tp: 8 (over x, core).
Axes of the slice: x: 4, y: 8, z: 8, core: 2. Of those that a mesh axis runs over, the one named last changes fastest.
Arguments:
- resid: bfloat16 [32768, 2048], P('sp'), may hold values from -6 to 6
- queries: bfloat16 [32768, 2048], P('sp', 'tp'), may hold values from -6 to 6
- keys: bfloat16 [32768, 512], P('sp', 'tp'), may hold values from -6 to 6
- values: bfloat16 [32768, 512], P('sp', 'tp'), may hold values from -6 to 6
- documents: int32 [32768], P('sp'), may hold values from 0 to 31, never falling along the last dimension, each value on 1 to 2048 neighbouring positions
- q_gain: float32 [64], replicated, may hold values from 0.5 to 6.5
- k_gain: float32 [64], replicated, may hold values from 0.5 to 6.5
- sink: float32 [32], P('tp'), may hold values from -1 to 5
- w_out: bfloat16 [2048, 2048], P('tp'), may hold values from -0.5 to 0.5
- n_gain: float32 [2048], replicated, may hold values from 0.1 to 1.9
- w_up: bfloat16 [2048, 8192], P('sp', 'tp'), may hold values from -0.125 to 0.125
- w_down: bfloat16 [8192, 2048], P('tp', 'sp'), may hold values from -0.0625 to 0.0625
Outputs:
- layer_out: bfloat16 [32768, 2048], P('sp')
All inputs are finite; a program needn't handle non-finite values.
Results may differ from a plain program's by a relative error of at most 0.018.
The roundings to bfloat16 on the way count: a program that leaves them out, or rounds other values in their place, can miss the bound.
Values may be sent and summed in bfloat16 or wider, within the bound.
A program may use at most 64 MiB of HBM per device.

v0:
```python
import jax
import jax.numpy as jnp
from jax import lax
from jax.sharding import PartitionSpec as P

WINDOW = 128
EPS = 1e-06


def gather_turned(arrays, axis, dims):
    turned = [jnp.moveaxis(a, dim, 0) for a, dim in zip(arrays, dims)]
    both = jnp.concatenate([t.reshape(len(t), -1) for t in turned], axis=1)
    result, at, outs = (lax.all_gather(both, axis, axis=0, tiled=True), 0, [])
    for t, dim in zip(turned, dims):
        section = result[:, at : at + t[0].size].reshape(-1, *t.shape[1:])
        outs.append(jnp.moveaxis(section, 0, dim))
        at += t[0].size
    return tuple(outs)


def extended(x, sides, width):
    for axis, dim in sides:
        count, length = (lax.axis_size(axis), x.shape[dim])
        up = [(i, (i + 1) % count) for i in range(count - 1)]
        down = [(j, i) for i, j in up]
        last = lax.slice_in_dim(x, length - width, length, axis=dim)
        initial = lax.slice_in_dim(x, 0, width, axis=dim)
        before = lax.ppermute(last, axis, up)
        after = lax.ppermute(initial, axis, down)
        x = jnp.concatenate([before, x, after], axis=dim)
    return x


def in_blocks(x, dim, count):
    dims = x.shape
    tiles = x.reshape(*dims[:dim], count, dims[dim] // count, *dims[dim + 1 :])
    return jnp.moveaxis(tiles, dim, 0)


def summed_on_arrival(x, axis, dim):
    count = lax.axis_size(axis)
    tiles = lax.all_to_all(in_blocks(x, dim, count), axis, 0, 0, tiled=True)
    return jnp.sum(tiles.astype(jnp.float32), axis=0)


def joined_along(tiles, dim):
    dims = list(tiles.shape[1:])
    dims[dim] *= tiles.shape[0]
    return jnp.moveaxis(tiles, 0, dim).reshape(dims)


def copy_for_each(x, axis):
    copies = jnp.broadcast_to(x, (lax.axis_size(axis), *x.shape))
    return lax.all_to_all(copies, axis, split_axis=0, concat_axis=0, tiled=True)


def collect(x, axis, dim):
    return joined_along(copy_for_each(x, axis), dim)


def rms_scale(field, gain):
    wide = field.astype(jnp.float32)
    return wide * lax.rsqrt(jnp.mean(wide * wide, axis=-1, keepdims=True) + EPS) * gain


def mixer_partial(normed, gathered):
    upward = jnp.dot(normed, gathered[0], preferred_element_type=jnp.float32)
    active = jnp.square(jax.nn.relu(upward)).astype(jnp.bfloat16)
    return jnp.dot(active, gathered[1], preferred_element_type=jnp.float32)


def shards(
    resid, queries, keys, values, documents, q_gain, k_gain, sink, w_out, n_gain, w_up, w_down
):
    rows = resid.shape[0]
    head_size = q_gain.shape[0]
    heads_here = sink.shape[0]
    kv_here = keys.shape[1] // head_size
    group = heads_here // kv_here
    gathered = None
    gathered = gather_turned((w_up, w_down), "sp", (0, 1))
    qnorm = rms_scale(queries.reshape(rows, kv_here, group, head_size), q_gain).astype(jnp.bfloat16)
    knorm = rms_scale(keys.reshape(rows, kv_here, head_size), k_gain).astype(jnp.bfloat16)
    vheads = values.reshape(rows, kv_here, head_size)
    doc_here = documents.astype(jnp.bfloat16)
    near_keys, near_values, near_docs = (
        extended(knorm, (("sp", 0),), WINDOW),
        extended(vheads, (("sp", 0),), WINDOW),
        extended(doc_here, (("sp", 0),), WINDOW),
    )
    offset = lax.axis_index("sp") * rows
    total = rows * lax.axis_size("sp")
    query_pos = offset + jnp.arange(rows, dtype=jnp.int32)
    key_pos = offset - WINDOW + jnp.arange(rows + 2 * WINDOW, dtype=jnp.int32)
    distance = key_pos[None, :] - query_pos[:, None]
    allowed = (jnp.abs(distance) <= WINDOW) & (key_pos[None, :] >= 0) & (key_pos[None, :] < total)
    allowed = allowed & (near_docs[None, :] == doc_here[:, None])
    heads_all = heads_here * lax.axis_size("tp")
    first_head = (lax.axis_index("tp") * heads_here).astype(jnp.float32)
    slopes = jnp.exp2(
        -8.0 * (first_head + jnp.arange(heads_here, dtype=jnp.float32) + 1.0) / heads_all
    )
    slopes = slopes.reshape(kv_here, group)
    sink_f = sink.reshape(kv_here, group)
    scores = jnp.einsum(
        "rkgd,skd->kgrs", qnorm, near_keys, preferred_element_type=jnp.float32
    ) * head_size ** (-0.5)
    scores = scores - slopes[:, :, None, None] * jnp.abs(distance).astype(jnp.float32)[None, None]
    scores = jnp.where(allowed[None, None], scores, jnp.float32(-1e30))
    highest = jnp.maximum(jnp.max(scores, axis=-1), sink_f[:, :, None])
    weights = jnp.exp(scores - highest[..., None])
    denom = jnp.sum(weights, axis=-1) + jnp.exp(sink_f[:, :, None] - highest)
    summed = jnp.einsum(
        "kgrs,skd->rkgd",
        weights.astype(jnp.bfloat16),
        near_values,
        preferred_element_type=jnp.float32,
    )
    attended = (
        (summed / denom.transpose(2, 0, 1)[..., None])
        .astype(jnp.bfloat16)
        .reshape(rows, heads_here * head_size)
    )
    share = rows // lax.axis_size("tp")
    head_mix = summed_on_arrival(
        jnp.dot(attended, w_out, preferred_element_type=jnp.float32).astype(jnp.bfloat16), "tp", 0
    )
    own_resid = lax.dynamic_slice_in_dim(resid, lax.axis_index("tp") * share, share, 0)
    middle = (own_resid.astype(jnp.float32) + head_mix).astype(jnp.bfloat16)
    normed_part = rms_scale(middle, n_gain).astype(jnp.bfloat16)
    normed = collect(normed_part, "tp", 0)
    partial_sum = mixer_partial(normed, gathered)
    unit_mix = summed_on_arrival(partial_sum.astype(jnp.bfloat16), "tp", 0)
    finished = (middle.astype(jnp.float32) + unit_mix).astype(jnp.bfloat16)
    return collect(finished, "tp", 0)


def solution(mesh):
    placed = (
        P("sp", None),
        P("sp", "tp"),
        P("sp", "tp"),
        P("sp", "tp"),
        P("sp"),
        P(),
        P(),
        P("tp"),
        P("tp", None),
        P(),
        P("sp", "tp"),
        P("tp", "sp"),
    )
    return jax.shard_map(
        shards, mesh=mesh, in_specs=placed, out_specs=P("sp", None), check_vma=False
    )
```

profile of v0, /device:TPU:1, one launch (start us, length us, event | category | flops | bytes accessed | tf_op | source)
XLA Modules:
  0.0 194.1 jit_solution(1907560911907022125)
XLA Ops:
  6.5 1.6 pad_maximum_fusion
  8.9 4.0 %collective-permute-start.2 = (bf16[128]{0:T(256)(128)(2,1)S(1)}, bf16[128]{0:T(256)(128)(2,1)S(1)}, u32[]{:S(2)}, u32[]{:S(2)}) collective-permute-start(bf16[128]{0:T(256)(128)(2,1)S(1)} %get-tuple-element.11), channel_id=1, source_target_pairs={{0,8},{8,16},{16,24},{24,32},{32,40},{40,48},{48,56},{56,64},{64,7... | collective-permute-start | bytes 776 | tf_op jit(solution)/shard_map/ppermute | solution.py:28
  12.9 1.3 collective-permute-start.3
  15.1 0.9 fusion.41
  16.0 4.0 %collective-permute-start.4 = (bf16[128,1,64]{0,2,1:T(8,128)(2,1)S(1)}, bf16[128,1,64]{0,2,1:T(8,128)(2,1)S(1)}, u32[]{:S(2)}, u32[]{:S(2)}) collective-permute-start(bf16[128,1,64]{0,2,1:T(8,128)(2,1)S(1)} %get-tuple-element.9), channel_id=1, source_target_pairs={{0,8},{8,16},{16,24},{24,32},{32,40},{40,48},{48,56},{56,64},{64,7... | collective-permute-start | bytes 49160 | tf_op jit(solution)/shard_map/ppermute | solution.py:28
  20.0 1.3 collective-permute-start.5
  22.1 4.0 %collective-permute-start = (bf16[128,1,64]{0,2,1:T(8,128)(2,1)S(1)}, bf16[128,1,64]{0,2,1:T(8,128)(2,1)S(1)}, u32[]{:S(2)}, u32[]{:S(2)}) collective-permute-start(bf16[128,1,64]{0,2,1:T(8,128)(2,1)S(1)} %get-tuple-element.7), channel_id=1, source_target_pairs={{0,8},{8,16},{16,24},{24,32},{32,40},{40,48},{48,56},{56,64},{64,7... | collective-permute-start | bytes 49160 | tf_op jit(solution)/shard_map/ppermute | solution.py:28
  26.1 1.1 copy.15
  27.3 0.9 fusion.67
  29.4 1.3 collective-permute-start.1
  30.8 1.0 fusion.20
  31.8 1.9 fusion.7
  33.8 1.9 fusion.1
  35.8 2.3 %fusion.30 = bf16[512,1,4,64]{0,3,2,1:T(8,128)(2,1)S(1)} fusion(f32[768,512,4]{1,0,2:T(8,128)S(1)} %get-tuple-element.14, f32[4,512]{1,0:T(4,128)S(1)} %broadcast_maximum_fusion, f32[512,768]{0,1:T(8,128)S(1)} %fusion.16, f32[4]{0:T(128)S(1)} %multiply_exponential_fusion, pred[512,768]{0,1:T(8,128)(4,1)S(1)} %fusion.20, f32[512,4]{0,1:T(4,128)S(1)} %fusion.54, ...), kind=kOutput, calls=%fused_computation.26 | convolution fusion | flops 211320832 | bytes 8634384 | tf_op jit(solution)/shard_map/kgrs,skd->rkgd/dot_general | solution.py:113
  38.1 2.1 %convolution_convert_fusion = bf16[512,2048]{1,0:T(8,128)(2,1)} fusion(bf16[512,256]{0,1:T(8,128)(2,1)S(1)} %bitcast.93, bf16[256,2048]{1,0:T(8,128)(2,1)S(1)} %copy-done), kind=kOutput, calls=%fused_computation.15 | convolution fusion | flops 537919488 | bytes 3407872 | tf_op jit(solution)/shard_map/dot_general | solution.py:126
  40.2 8.9 %all-to-all-start = ((bf16[8,64,2048]{2,1,0:T(8,128)(2,1)}), bf16[8,64,2048]{2,1,0:T(8,128)(2,1)S(1)}, u32[]{:S(2)}, u32[]{:S(2)}) async-start(bf16[8,64,2048]{2,1,0:T(8,128)(2,1)} %bitcast.23), calls=%async_computation | async-start | bytes 4194304 | tf_op jit(solution)/shard_map/all_to_all | solution.py:42
  49.0 26.2 %all-to-all-done = bf16[8,64,2048]{2,1,0:T(8,128)(2,1)S(1)} async-done(((bf16[8,64,2048]{2,1,0:T(8,128)(2,1)}), bf16[8,64,2048]{2,1,0:T(8,128)(2,1)S(1)}, u32[]{:S(2)}, u32[]{:S(2)}) %all-to-all-start) | async-done | bytes 2097184 | tf_op jit(solution)/shard_map/all_to_all | solution.py:42
  75.6 1.1 fusion.35
  77.2 29.6 %all_to_all.20 = bf16[8,64,2048]{2,1,0:T(8,128)(2,1)S(1)} all-to-all(bf16[8,64,2048]{2,1,0:T(8,128)(2,1)S(1)} %broadcast_in_dim.14), channel_id=1, replica_groups=mesh['sp'=64,'tp'=8] {'tp'}, dimensions={0} | all-to-all | bytes 4194304 | tf_op jit(solution)/shard_map/all_to_all | solution.py:54
  106.8 8.1 %all-gather.2.cloned.1.call-done = bf16[2048,2048]{1,0:T(8,128)(2,1)} async-done(((bf16[32,2048]{1,0:T(8,128)(2,1)}), bf16[2048,2048]{1,0:T(8,128)(2,1)}) %all-gather.2.cloned.1.call-update) | async-done | bytes 8388624 | tf_op jit(solution)/shard_map/all_gather | solution.py:13
  115.0 9.3 %fusion.11 = bf16[512,2048]{1,0:T(8,128)(2,1)} fusion(bf16[2048,2048]{1,0:T(8,128)(2,1)} %all-gather.2.cloned.1.call-done, bf16[512,2048]{1,0:T(8,128)(2,1)S(1)} %bitcast.91), kind=kOutput, calls=%fused_computation.14 | convolution fusion | flops 4297588736 | bytes 12582912 | tf_op jit(solution)/shard_map/dot_general | solution.py:69
  124.3 31.3 %all_to_all.21 = bf16[8,64,2048]{2,1,0:T(8,128)(2,1)S(1)} all-to-all(bf16[8,64,2048]{2,1,0:T(8,128)(2,1)} %bitcast.92), channel_id=1, replica_groups=mesh['sp'=64,'tp'=8] {'tp'}, dimensions={0} | all-to-all | bytes 4194304 | tf_op jit(solution)/shard_map/all_to_all | solution.py:42
  156.3 29.7 %all_to_all.22 = bf16[8,64,2048]{2,1,0:T(8,128)(2,1)S(1)} all-to-all(bf16[8,64,2048]{2,1,0:T(8,128)(2,1)S(1)} %broadcast_in_dim.15), channel_id=1, replica_groups=mesh['sp'=64,'tp'=8] {'tp'}, dimensions={0} | all-to-all | bytes 4194304 | tf_op jit(solution)/shard_map/all_to_all | solution.py:54
  186.0 1.3 copy.19
  (42 shorter events, 5.2 us)
Async XLA Ops:
  6.5 31.6 %copy-start = (bf16[256,2048]{1,0:T(8,128)(2,1)S(1)}, bf16[256,2048]{1,0:T(8,128)(2,1)}, u32[]{:S(2)}) copy-start(bf16[256,2048]{1,0:T(8,128)(2,1)} %param.20) | copy-start | bytes 3145732
  6.5 108.4 %all-gather.2.cloned.1.call-start = ((), (), s32[]{:S(2)}) async-start(), calls=%async_computation.4 | async-start | bytes 8519680 | tf_op jit(solution)/shard_map/all_gather | solution.py:13
  8.9 20.5 %collective-permute-start.2 = (bf16[128]{0:T(256)(128)(2,1)S(1)}, bf16[128]{0:T(256)(128)(2,1)S(1)}, u32[]{:S(2)}, u32[]{:S(2)}) collective-permute-start(bf16[128]{0:T(256)(128)(2,1)S(1)} %get-tuple-element.11), channel_id=1, source_target_pairs={{0,8},{8,16},{16,24},{24,32},{32,40},{40,48},{48,56},{56,64},{64,7... | collective-permute-start | bytes 776 | tf_op jit(solution)/shard_map/ppermute | solution.py:28
  12.9 17.8 %collective-permute-start.3 = (bf16[128]{0:T(256)(128)(2,1)S(1)}, bf16[128]{0:T(256)(128)(2,1)S(1)}, u32[]{:S(2)}, u32[]{:S(2)}) collective-permute-start(bf16[128]{0:T(256)(128)(2,1)S(1)} %get-tuple-element.12), channel_id=1, source_target_pairs={{8,0},{16,8},{24,16},{32,24},{40,32},{48,40},{56,48},{64,56},{72,6... | collective-permute-start | bytes 776 | tf_op jit(solution)/shard_map/ppermute | solution.py:29
  16.0 15.7 %collective-permute-start.4 = (bf16[128,1,64]{0,2,1:T(8,128)(2,1)S(1)}, bf16[128,1,64]{0,2,1:T(8,128)(2,1)S(1)}, u32[]{:S(2)}, u32[]{:S(2)}) collective-permute-start(bf16[128,1,64]{0,2,1:T(8,128)(2,1)S(1)} %get-tuple-element.9), channel_id=1, source_target_pairs={{0,8},{8,16},{16,24},{24,32},{32,40},{40,48},{48,56},{56,64},{64,7... | collective-permute-start | bytes 49160 | tf_op jit(solution)/shard_map/ppermute | solution.py:28
  20.0 11.8 %collective-permute-start.5 = (bf16[128,1,64]{0,2,1:T(8,128)(2,1)S(1)}, bf16[128,1,64]{0,2,1:T(8,128)(2,1)S(1)}, u32[]{:S(2)}, u32[]{:S(2)}) collective-permute-start(bf16[128,1,64]{0,2,1:T(8,128)(2,1)S(1)} %get-tuple-element.10), channel_id=1, source_target_pairs={{8,0},{16,8},{24,16},{32,24},{40,32},{48,40},{56,48},{64,56},{72,6... | collective-permute-start | bytes 49160 | tf_op jit(solution)/shard_map/ppermute | solution.py:29
  22.1 13.7 %collective-permute-start = (bf16[128,1,64]{0,2,1:T(8,128)(2,1)S(1)}, bf16[128,1,64]{0,2,1:T(8,128)(2,1)S(1)}, u32[]{:S(2)}, u32[]{:S(2)}) collective-permute-start(bf16[128,1,64]{0,2,1:T(8,128)(2,1)S(1)} %get-tuple-element.7), channel_id=1, source_target_pairs={{0,8},{8,16},{16,24},{24,32},{32,40},{40,48},{48,56},{56,64},{64,7... | collective-permute-start | bytes 49160 | tf_op jit(solution)/shard_map/ppermute | solution.py:28
  29.4 6.3 %collective-permute-start.1 = (bf16[128,1,64]{0,2,1:T(8,128)(2,1)S(1)}, bf16[128,1,64]{0,2,1:T(8,128)(2,1)S(1)}, u32[]{:S(2)}, u32[]{:S(2)}) collective-permute-start(bf16[128,1,64]{0,2,1:T(8,128)(2,1)S(1)} %get-tuple-element.8), channel_id=1, source_target_pairs={{8,0},{16,8},{24,16},{32,24},{40,32},{48,40},{56,48},{64,56},{72,6... | collective-permute-start | bytes 49160 | tf_op jit(solution)/shard_map/ppermute | solution.py:29
  31.8 1.9 copy-start.3
  33.7 2.1 %copy-start.1 = (bf16[512,64]{0,1:T(8,128)(2,1)S(1)}, bf16[512,64]{0,1:T(8,128)(2,1)}, u32[]{:S(2)}) copy-start(bf16[512,64]{0,1:T(8,128)(2,1)} %param.15) | copy-start | bytes 196612
  40.2 36.6 %copy-start.2 = (f32[2048]{0:T(1024)S(1)}, f32[2048]{0:T(1024)}, u32[]{:S(2)}) copy-start(f32[2048]{0:T(1024)} %param.21) | copy-start | bytes 24580
  40.2 35.1 %all-to-all-start = ((bf16[8,64,2048]{2,1,0:T(8,128)(2,1)}), bf16[8,64,2048]{2,1,0:T(8,128)(2,1)S(1)}, u32[]{:S(2)}, u32[]{:S(2)}) async-start(bf16[8,64,2048]{2,1,0:T(8,128)(2,1)} %bitcast.23), calls=%async_computation | async-start | bytes 4194304 | tf_op jit(solution)/shard_map/all_to_all | solution.py:42
Sparse Core Ops, SparseCore 0:
  10.4 104.5 all-gather.1
where the time goes:
time: 195 us; the launch traced here: 194 us
  blocking collectives  90.6 us (46%)
  waiting for transfers between devices  34.4 us (18%)
  starting transfers between devices  24.7 us (13%)
  matrix products  15.6 us (8%)
  between operations  13.7 us (7%)
  other arithmetic  10.7 us (5%)
  local copies, waits for them, and re-layouts  4.41 us (2%)
    all_to_all x2, blocking collectives, copy_for_each(): return lax.all_to_all(copies, axis, split_axis=0, concat_axis=0, tiled=True)  59.3 us
    all_to_all x1, blocking collectives, summed_on_arrival(): tiles = lax.all_to_all(in_blocks(x, dim, count), axis, 0, 0, tiled=True)  31.3 us
    all_to_all x1, waiting for transfers between devices, summed_on_arrival(): tiles = lax.all_to_all(in_blocks(x, dim, count), axis, 0, 0, tiled=True)  26.2 us
    ppermute x3, starting transfers between devices, extended(): before = lax.ppermute(last, axis, up)  12 us
    dot_general x1, matrix products, mixer_partial(): return jnp.dot(active, gathered[1], preferred_element_type=jnp.float32)  9.31 us
    all_to_all x1, starting transfers between devices, summed_on_arrival(): tiles = lax.all_to_all(in_blocks(x, dim, count), axis, 0, 0, tiled=True)  8.88 us
    all_gather x1, waiting for transfers between devices, gather_turned(): result, at, outs = (lax.all_gather(both, axis, axis=0, tiled=True), 0, [])  8.14 us
  transfers between devices with their start and end apart: 8, of which 2 were waited for; matrix products, arithmetic and copies ran while one was open for 9% of the time, Pallas kernels for 0%

commit v1 on v0

--- a/solution.py
+++ b/solution.py
@@ -7,10 +7,15 @@
 EPS = 1e-06
 
 
+def gather_over(x, name, d):
+    sent = jnp.stack([x] * lax.axis_size(name))
+    return jnp.concatenate(lax.all_to_all(sent, name, 0, 0), axis=d)
+
+
 def gather_turned(arrays, axis, dims):
     turned = [jnp.moveaxis(a, dim, 0) for a, dim in zip(arrays, dims)]
     both = jnp.concatenate([t.reshape(len(t), -1) for t in turned], axis=1)
-    result, at, outs = (lax.all_gather(both, axis, axis=0, tiled=True), 0, [])
+    result, at, outs = (gather_over(both, axis, 0), 0, [])
     for t, dim in zip(turned, dims):
         section = result[:, at : at + t[0].size].reshape(-1, *t.shape[1:])
         outs.append(jnp.moveaxis(section, 0, dim))

time: 195 us -> 394 us (2.02)
  the two profiles are of different devices: /device:TPU:1 before, /device:TPU:32 now
where the time goes in v1:
time: 394 us; the launch traced here: 393 us
  blocking collectives  281 us (71%)
  waiting for transfers between devices  53.4 us (14%)
  starting transfers between devices  26.4 us (7%)
  matrix products  15.6 us (4%)
  other arithmetic  10 us (3%)
  local copies, waits for them, and re-layouts  6.8 us (2%)
    all_to_all x1, blocking collectives, gather_over(): return jnp.concatenate(lax.all_to_all(sent, name, 0, 0), axis=d)  212 us
    all_to_all x1, blocking collectives, summed_on_arrival(): tiles = lax.all_to_all(in_blocks(x, dim, count), axis, 0, 0, tiled=True)  39.6 us
    all_to_all x1, blocking collectives, copy_for_each(): return lax.all_to_all(copies, axis, split_axis=0, concat_axis=0, tiled=True)  29.7 us
    all_to_all x1, waiting for transfers between devices, summed_on_arrival(): tiles = lax.all_to_all(in_blocks(x, dim, count), axis, 0, 0, tiled=True)  27.2 us
    all_to_all x1, waiting for transfers between devices, copy_for_each(): return lax.all_to_all(copies, axis, split_axis=0, concat_axis=0, tiled=True)  26.2 us
    ppermute x3, starting transfers between devices, extended(): after = lax.ppermute(initial, axis, down)  10.7 us
    dot_general x1, matrix products, mixer_partial(): return jnp.dot(active, gathered[1], preferred_element_type=jnp.float32)  9.28 us
  transfers between devices with their start and end apart: 8, of which 2 were waited for; matrix products, arithmetic and copies ran while one was open for 3% of the time, Pallas kernels for 0%

profile of v1, /device:TPU:32, one launch (start us, length us, event | category | flops | bytes accessed | tf_op | source)
XLA Modules:
  0.0 393.5 jit_solution(11134831291357981238)
XLA Ops:
  0.8 2.3 collective-permute-start.3
  3.1 3.5 collective-permute-start.2
  8.5 3.6 collective-permute-start.5
  12.0 2.3 collective-permute-start.4
  15.1 4.8 %collective-permute-start.1 = (bf16[128,1,64]{0,2,1:T(8,128)(2,1)S(1)}, bf16[128,1,64]{0,2,1:T(8,128)(2,1)S(1)}, u32[]{:S(2)}, u32[]{:S(2)}) collective-permute-start(bf16[128,1,64]{0,2,1:T(8,128)(2,1)S(1)} %get-tuple-element.8), channel_id=1, source_target_pairs={{8,0},{16,8},{24,16},{32,24},{40,32},{48,40},{56,48},{64,56},{72,6... | collective-permute-start | bytes 49160 | tf_op jit(solution)/shard_map/ppermute | solution.py:34
  20.8 1.1 copy.15
  23.2 1.9 collective-permute-start
  25.2 1.0 fusion.20
  26.2 1.9 fusion.7
  28.2 1.9 fusion.1
  30.2 2.3 fusion.30
  32.5 2.1 convolution_convert_fusion
  34.6 4.4 %all-to-all-start = ((bf16[8,64,2048]{2,1,0:T(8,128)(2,1)}), bf16[8,64,2048]{2,1,0:T(8,128)(2,1)S(1)}, u32[]{:S(2)}, u32[]{:S(2)}) async-start(bf16[8,64,2048]{2,1,0:T(8,128)(2,1)} %bitcast.23), calls=%async_computation | async-start | bytes 4194304 | tf_op jit(solution)/shard_map/all_to_all | solution.py:47
  39.0 27.2 %all-to-all-done = bf16[8,64,2048]{2,1,0:T(8,128)(2,1)S(1)} async-done(((bf16[8,64,2048]{2,1,0:T(8,128)(2,1)}), bf16[8,64,2048]{2,1,0:T(8,128)(2,1)S(1)}, u32[]{:S(2)}, u32[]{:S(2)}) %all-to-all-start) | async-done | bytes 2097184 | tf_op jit(solution)/shard_map/all_to_all | solution.py:47
  66.6 1.1 fusion.35
  67.9 1.6 broadcast_in_dim.14
  69.4 3.6 all-to-all-start.1
  73.9 26.2 %all-to-all-done.1 = bf16[8,64,2048]{2,1,0:T(8,128)(2,1)S(1)} async-done(((bf16[8,64,2048]{2,1,0:T(8,128)(2,1)}), bf16[8,64,2048]{2,1,0:T(8,128)(2,1)S(1)}, u32[]{:S(2)}, u32[]{:S(2)}) %all-to-all-start.1) | async-done | bytes 2097184 | tf_op jit(solution)/shard_map/all_to_all | solution.py:59
  100.1 1.1 stack.2
  101.2 211.7 %all_to_all.25 = bf16[64,32,2048]{2,1,0:T(8,128)(2,1)} all-to-all(bf16[64,32,2048]{2,1,0:T(8,128)(2,1)S(1)} %stack.2), channel_id=1, replica_groups=mesh['sp'=64,'tp'=8] {'sp'}, dimensions={0} | all-to-all | bytes 16777216 | tf_op jit(solution)/shard_map/all_to_all | solution.py:12
  312.9 9.3 %fusion.11 = bf16[512,2048]{1,0:T(8,128)(2,1)} fusion(bf16[2048,2048]{1,0:T(8,128)(2,1)} %bitcast.91, bf16[512,2048]{1,0:T(8,128)(2,1)S(1)} %bitcast.93), kind=kOutput, calls=%fused_computation.14 | convolution fusion | flops 4297588736 | bytes 12582912 | tf_op jit(solution)/shard_map/dot_general | solution.py:74
  322.2 39.6 %all_to_all.26 = bf16[8,64,2048]{2,1,0:T(8,128)(2,1)S(1)} all-to-all(bf16[8,64,2048]{2,1,0:T(8,128)(2,1)} %bitcast.94), channel_id=1, replica_groups=mesh['sp'=64,'tp'=8] {'tp'}, dimensions={0} | all-to-all | bytes 4194304 | tf_op jit(solution)/shard_map/all_to_all | solution.py:47
  362.5 29.7 %all_to_all.27 = bf16[8,64,2048]{2,1,0:T(8,128)(2,1)S(1)} all-to-all(bf16[8,64,2048]{2,1,0:T(8,128)(2,1)S(1)} %broadcast_in_dim.15), channel_id=1, replica_groups=mesh['sp'=64,'tp'=8] {'tp'}, dimensions={0} | all-to-all | bytes 4194304 | tf_op jit(solution)/shard_map/all_to_all | solution.py:59
  392.1 1.3 copy.19
  (42 shorter events, 7.8 us)
Async XLA Ops:
  0.0 32.5 %copy-start = (bf16[256,2048]{1,0:T(8,128)(2,1)S(1)}, bf16[256,2048]{1,0:T(8,128)(2,1)}, u32[]{:S(2)}) copy-start(bf16[256,2048]{1,0:T(8,128)(2,1)} %param.20) | copy-start | bytes 3145732
  0.8 22.4 %collective-permute-start.3 = (bf16[128]{0:T(256)(128)(2,1)S(1)}, bf16[128]{0:T(256)(128)(2,1)S(1)}, u32[]{:S(2)}, u32[]{:S(2)}) collective-permute-start(bf16[128]{0:T(256)(128)(2,1)S(1)} %get-tuple-element.12), channel_id=1, source_target_pairs={{8,0},{16,8},{24,16},{32,24},{40,32},{48,40},{56,48},{64,56},{72,6... | collective-permute-start | bytes 776 | tf_op jit(solution)/shard_map/ppermute | solution.py:34
  3.1 22.0 %collective-permute-start.2 = (bf16[128]{0:T(256)(128)(2,1)S(1)}, bf16[128]{0:T(256)(128)(2,1)S(1)}, u32[]{:S(2)}, u32[]{:S(2)}) collective-permute-start(bf16[128]{0:T(256)(128)(2,1)S(1)} %get-tuple-element.11), channel_id=1, source_target_pairs={{0,8},{8,16},{16,24},{24,32},{32,40},{40,48},{48,56},{56,64},{64,7... | collective-permute-start | bytes 776 | tf_op jit(solution)/shard_map/ppermute | solution.py:33
  8.5 17.7 %collective-permute-start.5 = (bf16[128,1,64]{0,2,1:T(8,128)(2,1)S(1)}, bf16[128,1,64]{0,2,1:T(8,128)(2,1)S(1)}, u32[]{:S(2)}, u32[]{:S(2)}) collective-permute-start(bf16[128,1,64]{0,2,1:T(8,128)(2,1)S(1)} %get-tuple-element.10), channel_id=1, source_target_pairs={{8,0},{16,8},{24,16},{32,24},{40,32},{48,40},{56,48},{64,56},{72,6... | collective-permute-start | bytes 49160 | tf_op jit(solution)/shard_map/ppermute | solution.py:34
  12.0 14.2 %collective-permute-start.4 = (bf16[128,1,64]{0,2,1:T(8,128)(2,1)S(1)}, bf16[128,1,64]{0,2,1:T(8,128)(2,1)S(1)}, u32[]{:S(2)}, u32[]{:S(2)}) collective-permute-start(bf16[128,1,64]{0,2,1:T(8,128)(2,1)S(1)} %get-tuple-element.9), channel_id=1, source_target_pairs={{0,8},{8,16},{16,24},{24,32},{32,40},{40,48},{48,56},{56,64},{64,7... | collective-permute-start | bytes 49160 | tf_op jit(solution)/shard_map/ppermute | solution.py:33
  15.1 15.1 %collective-permute-start.1 = (bf16[128,1,64]{0,2,1:T(8,128)(2,1)S(1)}, bf16[128,1,64]{0,2,1:T(8,128)(2,1)S(1)}, u32[]{:S(2)}, u32[]{:S(2)}) collective-permute-start(bf16[128,1,64]{0,2,1:T(8,128)(2,1)S(1)} %get-tuple-element.8), channel_id=1, source_target_pairs={{8,0},{16,8},{24,16},{32,24},{40,32},{48,40},{56,48},{64,56},{72,6... | collective-permute-start | bytes 49160 | tf_op jit(solution)/shard_map/ppermute | solution.py:34
  23.2 6.9 %collective-permute-start = (bf16[128,1,64]{0,2,1:T(8,128)(2,1)S(1)}, bf16[128,1,64]{0,2,1:T(8,128)(2,1)S(1)}, u32[]{:S(2)}, u32[]{:S(2)}) collective-permute-start(bf16[128,1,64]{0,2,1:T(8,128)(2,1)S(1)} %get-tuple-element.7), channel_id=1, source_target_pairs={{0,8},{8,16},{16,24},{24,32},{32,40},{40,48},{48,56},{56,64},{64,7... | collective-permute-start | bytes 49160 | tf_op jit(solution)/shard_map/ppermute | solution.py:33
  26.2 1.9 copy-start.3
  28.1 2.1 copy-start.1
  34.6 33.1 %copy-start.2 = (f32[2048]{0:T(1024)S(1)}, f32[2048]{0:T(1024)}, u32[]{:S(2)}) copy-start(f32[2048]{0:T(1024)} %param.21) | copy-start | bytes 24580
  34.6 31.6 %all-to-all-start = ((bf16[8,64,2048]{2,1,0:T(8,128)(2,1)}), bf16[8,64,2048]{2,1,0:T(8,128)(2,1)S(1)}, u32[]{:S(2)}, u32[]{:S(2)}) async-start(bf16[8,64,2048]{2,1,0:T(8,128)(2,1)} %bitcast.23), calls=%async_computation | async-start | bytes 4194304 | tf_op jit(solution)/shard_map/all_to_all | solution.py:47
  69.4 30.7 %all-to-all-start.1 = ((bf16[8,64,2048]{2,1,0:T(8,128)(2,1)}), bf16[8,64,2048]{2,1,0:T(8,128)(2,1)S(1)}, u32[]{:S(2)}, u32[]{:S(2)}) async-start(bf16[8,64,2048]{2,1,0:T(8,128)(2,1)} %broadcast_in_dim.14), calls=%async_computation.1 | async-start | bytes 4194304 | tf_op jit(solution)/shard_map/all_to_all | solution.py:59
